TPU v7x, 256 devices: a whole 4x4x8 slice. The times are simulated.
256 devices in a mesh: sp: 64 (over z, y, core), tp: 4 (over x).
Axes of the slice: x: 4, y: 4, z: 8, core: 2. Of those that a mesh axis runs over, the one named last changes fastest.
Arguments:
- out_grad: bfloat16 [12288, 2048], P('sp'), may hold values from -16 to 16
- routes: int32 [12288, 2], P('sp'), may hold values from 0 to 63, all different within a row; in each aligned block of 192 rows (0 to 191, 192 to 383, ...) at most 12 rows name the same one
- route_weight: float32 [12288, 2], P('sp'), may hold values from 0.3 to 1.5
- expert_rows: bfloat16 [64, 64, 12, 2048], P(None, 'sp'), may hold values from -6 to 6
- gate_weight: bfloat16 [64, 2048, 1024], P('sp', None, 'tp'), may hold values from -0.125 to 0.125
- up_weight: bfloat16 [64, 2048, 1024], P('sp', None, 'tp'), may hold values from -0.125 to 0.125
- down_weight: bfloat16 [64, 1024, 2048], P('sp', 'tp'), may hold values from -0.1875 to 0.1875
- conv_input: bfloat16 [12288, 1024], P('sp', 'tp'), may hold values from -6 to 6
- out_gate: bfloat16 [12288, 1024], P('sp', 'tp'), may hold values from -6 to 6
- in_gate: bfloat16 [12288, 1024], P('sp', 'tp'), may hold values from -6 to 6
- taps: float32 [3, 1024], P(None, 'tp'), may hold values from -3 to 3
- out_weight: bfloat16 [2048, 1024], P(None, 'tp'), may hold values from -0.1875 to 0.1875
Outputs:
- gate_grad: bfloat16 [64, 2048, 1024], P('sp', None, 'tp')
- up_grad: bfloat16 [64, 2048, 1024], P('sp', None, 'tp')
- down_grad: bfloat16 [64, 1024, 2048], P('sp', 'tp')
- mid_grad: bfloat16 [12288, 2048], P('sp', 'tp')
- out_weight_grad: float32 [2048, 1024], P('sp', 'tp')
- input_grad: bfloat16 [12288, 1024], P('sp', 'tp')
- out_gate_grad: bfloat16 [12288, 1024], P('sp', 'tp')
- in_gate_grad: bfloat16 [12288, 1024], P('sp', 'tp')
Inputs may be any that keep to these rules, and one draw needn't show every extreme that they name: `routes`: each token names 2 different experts; within each aligned block of 192 tokens no expert is named by more than 12 tokens, a bound that some block reaches.
All inputs are finite; a program needn't handle non-finite values.
Results may differ from a plain program's by a relative error of at most 0.014.
Values may be sent and summed in bfloat16 or wider, within the bound.
No kernel may reach another device: no remote copies, remote signals or barrier semaphores. Data moves between devices by JAX's collectives and lax.ppermute only.
A program may use at most 64 MiB of HBM per device.

v0:
```python
import jax
import jax.numpy as jnp
from jax import lax
from jax.sharding import PartitionSpec as P


def split_up(shard, dim, peers):
    shape = shard.shape
    pieces = shard.reshape(*shape[:dim], peers, shape[dim] // peers, *shape[dim + 1 :])
    return jnp.moveaxis(pieces, dim, 0)


def sum_at_owner(shard, axis, dim):
    peers = lax.axis_size(axis)
    pieces = lax.all_to_all(split_up(shard, dim, peers), axis, 0, 0, tiled=True)
    return jnp.sum(pieces.astype(jnp.float32), axis=0)


def passed_along(shard, axis, by):
    peers = lax.axis_size(axis)
    pairs = [(i, i + by) for i in range(peers) if 0 <= i + by < peers]
    return lax.ppermute(shard, axis, pairs)


def on_device(
    out_grad,
    routes,
    route_weight,
    expert_rows,
    gate_weight,
    up_weight,
    down_weight,
    conv_input,
    out_gate,
    in_gate,
    taps,
    out_weight,
):
    groups = lax.axis_size("tp")
    member = lax.axis_index("tp")
    sources = lax.axis_size("sp")
    tok_rows, width = out_grad.shape
    top = routes.shape[1]
    local = gate_weight.shape[0]
    experts = local * sources
    slots = expert_rows.shape[2]
    share = width // groups
    flat = routes.reshape(-1)
    onehot = (flat[:, None] == jnp.arange(experts, dtype=jnp.int32)[None, :]).astype(jnp.int32)
    place = jnp.sum((jnp.cumsum(onehot, axis=0) - onehot) * onehot, axis=1)
    target = flat * slots + place
    slot_grad = (route_weight[:, :, None] * out_grad[:, None, :].astype(jnp.float32)).astype(
        jnp.bfloat16
    )
    outgoing = (
        jnp.zeros((experts * slots, width), jnp.bfloat16)
        .at[target]
        .set(slot_grad.reshape(-1, width))
    )
    outgoing = outgoing.reshape(sources, local, slots, width)
    portion = slots // groups
    piece = lax.dynamic_slice_in_dim(outgoing, member * portion, portion, 2)
    arrived = lax.all_to_all(piece, "sp", split_axis=0, concat_axis=0, tiled=True)
    grads = lax.all_gather(arrived, "tp", axis=2, tiled=True)
    gate = jnp.einsum(
        "secd,edf->secf", expert_rows, gate_weight, preferred_element_type=jnp.float32
    )
    up = jnp.einsum("secd,edf->secf", expert_rows, up_weight, preferred_element_type=jnp.float32)
    sig = jax.nn.sigmoid(gate)
    act = (gate * sig * up).astype(jnp.bfloat16)
    act_grad = jnp.einsum("secd,efd->secf", grads, down_weight, preferred_element_type=jnp.float32)
    up_part = (act_grad * gate * sig).astype(jnp.bfloat16)
    gate_part = (act_grad * up * sig * (1.0 + gate * (1.0 - sig))).astype(jnp.bfloat16)
    down_grad = jnp.einsum("secf,secd->efd", act, grads, preferred_element_type=jnp.float32).astype(
        jnp.bfloat16
    )
    gate_grad = jnp.einsum(
        "secd,secf->edf", expert_rows, gate_part, preferred_element_type=jnp.float32
    ).astype(jnp.bfloat16)
    up_grad = jnp.einsum(
        "secd,secf->edf", expert_rows, up_part, preferred_element_type=jnp.float32
    ).astype(jnp.bfloat16)
    row_part = jnp.einsum(
        "secf,edf->secd", gate_part, gate_weight, preferred_element_type=jnp.float32
    )
    row_part = row_part + jnp.einsum(
        "secf,edf->secd", up_part, up_weight, preferred_element_type=jnp.float32
    )
    summed = sum_at_owner(row_part.astype(jnp.bfloat16), "tp", 3)
    returned = lax.all_to_all(
        summed.astype(jnp.bfloat16), "sp", split_axis=0, concat_axis=0, tiled=True
    )
    returned = returned.reshape(experts * slots, share)
    picked = (
        jnp.take(returned, target, axis=0)
        .astype(jnp.float32)
        .reshape(tok_rows, top, share)
        .sum(axis=1)
    )
    own_cols = lax.dynamic_slice_in_dim(out_grad, member * share, share, 1).astype(jnp.float32)
    mid_grad = (own_cols + picked).astype(jnp.bfloat16)
    mid_whole = lax.all_gather(mid_grad, "tp", axis=1, tiled=True)
    reach = taps.shape[0] - 1
    rims = jnp.stack([in_gate[tok_rows - reach :], conv_input[tok_rows - reach :]])
    prior = passed_along(rims, "sp", 1)
    mixed = in_gate.astype(jnp.float32) * conv_input.astype(jnp.float32)
    prior_mixed = prior[0].astype(jnp.float32) * prior[1].astype(jnp.float32)
    extended = jnp.concatenate([prior_mixed, mixed], axis=0)
    conv = jnp.zeros_like(mixed)
    for tap in range(reach + 1):
        conv = conv + taps[tap][None, :] * extended[reach - tap : reach - tap + tok_rows]
    gated = (out_gate.astype(jnp.float32) * conv).astype(jnp.bfloat16)
    out_weight_grad = sum_at_owner(
        lax.dot_general(
            mid_whole, gated, (((0,), (0,)), ((), ())), preferred_element_type=jnp.float32
        ).astype(jnp.bfloat16),
        "sp",
        0,
    )
    gated_grad = jnp.dot(mid_whole, out_weight, preferred_element_type=jnp.float32)
    out_gate_grad = (gated_grad * conv).astype(jnp.bfloat16)
    conv_grad = gated_grad * out_gate.astype(jnp.float32)
    later = passed_along(conv_grad[:reach], "sp", -1)
    following = jnp.concatenate([conv_grad, later], axis=0)
    mixed_grad = jnp.zeros_like(conv_grad)
    for tap in range(reach + 1):
        mixed_grad = mixed_grad + taps[tap][None, :] * following[tap : tap + tok_rows]
    input_grad = (mixed_grad * in_gate.astype(jnp.float32)).astype(jnp.bfloat16)
    in_gate_grad = (mixed_grad * conv_input.astype(jnp.float32)).astype(jnp.bfloat16)
    return (
        gate_grad,
        up_grad,
        down_grad,
        mid_grad,
        out_weight_grad,
        input_grad,
        out_gate_grad,
        in_gate_grad,
    )


def solution(mesh):
    in_specs = (
        P("sp", None),
        P("sp", None),
        P("sp", None),
        P(None, "sp", None, None),
        P("sp", None, "tp"),
        P("sp", None, "tp"),
        P("sp", "tp", None),
        P("sp", "tp"),
        P("sp", "tp"),
        P("sp", "tp"),
        P(None, "tp"),
        P(None, "tp"),
    )
    out_specs = (
        P("sp", None, "tp"),
        P("sp", None, "tp"),
        P("sp", "tp", None),
        P("sp", "tp"),
        P("sp", "tp"),
        P("sp", "tp"),
        P("sp", "tp"),
        P("sp", "tp"),
    )
    return jax.shard_map(
        on_device, mesh=mesh, in_specs=in_specs, out_specs=out_specs, check_vma=False
    )
```

profile of v0, /device:TPU:1, one launch (start us, length us, event | category | flops | bytes accessed | tf_op | source)
XLA Modules:
  0.0 281.8 jit_solution(15357142444350941405)
XLA Ops:
  10.7 4.4 %mul.148 = f32[192,2,2048]{2,1,0:T(2,128)} broadcast(bf16[192,2048]{1,0:T(8,128)(2,1)} %param.12), dimensions={0,2} | broadcast | bytes 3932160 | tf_op jit(solution)/shard_map/mul | solution.py:52
  15.1 5.3 %mul.149 = f32[384,2048]{1,0:T(8,128)} reshape(f32[192,2,2048]{2,1,0:T(2,128)} %mul.148) | data formatting | bytes 6291456 | tf_op jit(solution)/shard_map/mul | solution.py:52
  20.8 6.4 %scatter_custom_fusion = bf16[768,2048]{1,0:T(8,128)(2,1)} fusion(s32[384]{0:T(512)S(1)} %fusion.80, f32[384,2048]{1,0:T(8,128)} %mul.149, f32[384]{0:T(512)S(1)} %mul.146, bf16[]{:T(256)} %constant.12.clone.1), kind=kCustom, calls=%fused_computation.28 | custom fusion | flops 1572864 | bytes 6293506 | tf_op jit(solution)/shard_map/scatter | solution.py:58
  27.2 6.1 %reshape.145 = bf16[64,1,12,2048]{3,2,0,1:T(8,128)(2,1)} reshape(bf16[768,2048]{1,0:T(8,128)(2,1)} %scatter_custom_fusion) | data formatting | bytes 6291456 | tf_op jit(solution)/shard_map/reshape | solution.py:60
  33.2 3.0 %dynamic-slice_bitcast_fusion = bf16[64,1,3,2048]{3,2,1,0:T(4,128)(2,1)S(1)} fusion(bf16[64,1,12,2048]{3,2,0,1:T(8,128)(2,1)} %reshape.145, s32[]{:T(128)S(6)} %select_n.30), kind=kLoop, calls=%fused_computation.40 | loop fusion | bytes 1572868 | tf_op jit(solution)/shard_map/dynamic_slice | solution.py:62
  36.3 41.1 %all_to_all.20 = bf16[64,1,3,2048]{3,2,1,0:T(4,128)(2,1)S(1)} all-to-all(bf16[64,1,3,2048]{3,2,1,0:T(4,128)(2,1)S(1)} %dynamic-slice_bitcast_fusion), channel_id=1, replica_groups=mesh['sp'=64,'tp'=4] {'sp'}, dimensions={0} | all-to-all | bytes 1572864 | tf_op jit(solution)/shard_map/all_to_all | solution.py:63
  77.4 1.5 copy.49
  78.9 3.2 %fusion.48 = f32[64,1,12,256]{3,0,2,1:T(8,128)} fusion(bf16[64,1,12,2048]{3,0,2,1:T(8,128)(2,1)S(1)} %copy-done, bf16[1,2048,256]{2,1,0:T(8,128)(2,1)} %param.16), kind=kOutput, calls=%fused_computation.33 | convolution fusion | flops 805306368 | bytes 4980736 | tf_op jit(solution)/shard_map/secd,edf->secf/dot_general | solution.py:65
  82.1 1.9 fusion.45
  84.0 33.8 %all-gather.2.cloned.1.call-done = bf16[64,1,12,2048]{3,0,1,2:T(8,128)(2,1)} async-done(((bf16[64,1,3,2048]{3,0,1,2:T(8,128)(2,1)}), bf16[64,1,12,2048]{3,0,1,2:T(8,128)(2,1)}) %all-gather.2.cloned.1.call-update) | async-done | bytes 3145744 | tf_op jit(solution)/shard_map/all_gather | solution.py:64
  117.8 3.9 %multiply_convert_fusion.3 = (bf16[64,1,12,256]{3,0,2,1:T(8,128)(2,1)S(1)}, bf16[64,1,12,256]{3,0,2,1:T(8,128)(2,1)S(1)}) fusion(f32[64,1,12,256]{3,0,2,1:T(8,128)} %fusion.48, f32[64,1,12,256]{3,0,2,1:T(8,128)} %fusion.45, bf16[1,256,2048]{2,1,0:T(8,128)(2,1)} %param.18, bf16[64,1,12,2048]{3,0,1,2:T(8,128)(2,1)} %all-gather.2.cloned.1.call-done), kind=kOutput, calls=%fused_computation.43 | convolution fusion | flops 807862272 | bytes 6553600 | tf_op jit(solution)/shard_map/secd,efd->secf/dot_general | solution.py:71
  124.6 39.9 %all_to_all.21 = bf16[4,64,1,12,512]{4,1,3,2,0:T(8,128)(2,1)} all-to-all(bf16[4,64,1,12,512]{4,1,3,2,0:T(8,128)(2,1)S(1)} %bitcast.161), channel_id=1, replica_groups=mesh['sp'=64,'tp'=4] {'tp'}, dimensions={0} | all-to-all | bytes 6291456 | tf_op jit(solution)/shard_map/all_to_all | solution.py:15
  164.5 3.5 %reduce_sum.48 = bf16[64,12,512]{2,0,1:T(8,128)(2,1)} reduce(bf16[4,64,1,12,512]{4,1,3,2,0:T(8,128)(2,1)} %all_to_all.21, bf16[]{:T(256)} %constant.12.clone.1), dimensions={0,2}, to_apply=%region_4.5 | reduce | flops 1179648 | bytes 3932162 | tf_op jit(solution)/shard_map/reduce_sum | solution.py:16
  168.1 2.5 copy.54
  170.6 12.1 %all-to-all-start.2 = ((bf16[64,1,12,512]{3,2,1,0:T(8,128)(2,1)}), bf16[64,1,12,512]{3,2,1,0:T(8,128)(2,1)}, u32[]{:S(2)}, u32[]{:S(2)}) async-start(bf16[64,1,12,512]{3,2,1,0:T(8,128)(2,1)} %copy.54), calls=%async_computation.2 | async-start | bytes 2097152 | tf_op jit(solution)/shard_map/all_to_all | solution.py:90
  182.8 3.5 %collective-permute-start = (bf16[2,2,256]{2,1,0:T(2,128)(2,1)S(1)}, bf16[2,2,256]{2,1,0:T(2,128)(2,1)S(1)}, u32[]{:S(2)}, u32[]{:S(2)}) collective-permute-start(bf16[2,2,256]{2,1,0:T(2,128)(2,1)S(1)} %pad_maximum_fusion.2), channel_id=1, source_target_pairs={{0,4},{4,8},{8,12},{12,16},{16,20},{20,24},{24,28},{28,32},{32,36}... | collective-permute-start | bytes 6152 | tf_op jit(solution)/shard_map/ppermute | solution.py:22
  188.6 22.2 %all-to-all-done.2 = bf16[64,1,12,512]{3,2,1,0:T(8,128)(2,1)} async-done(((bf16[64,1,12,512]{3,2,1,0:T(8,128)(2,1)}), bf16[64,1,12,512]{3,2,1,0:T(8,128)(2,1)}, u32[]{:S(2)}, u32[]{:S(2)}) %all-to-all-start.2) | async-done | bytes 786464 | tf_op jit(solution)/shard_map/all_to_all | solution.py:90
  210.8 2.1 reshape.155
  212.9 3.3 %gather_fusion = bf16[384,512]{1,0:T(8,128)(2,1)S(1)} fusion(bf16[768,512]{1,0:T(8,128)(2,1)} %reshape.155, s32[1024]{0:T(1024)S(1)} %pad_clamp_fusion), kind=kCustom, calls=%fused_computation | custom fusion | bytes 787968 | tf_op jit(solution)/shard_map/jit(_take)/gather | solution.py:95
  217.1 2.2 convert_reduce_fusion.1
  220.3 11.0 %all_gather.7 = bf16[192,2048]{1,0:T(8,128)(2,1)S(1)} all-gather(bf16[192,512]{1,0:T(8,128)(2,1)S(1)} %add_convert_fusion.1), channel_id=1, replica_groups=mesh['sp'=64,'tp'=4] {'tp'}, dimensions={1}, use_global_device_ids=true | all-gather | bytes 983040 | tf_op jit(solution)/shard_map/all_gather | solution.py:102
  231.3 2.5 multiply_convert_fusion.6
  233.7 1.5 convolution_convert_fusion
  235.2 9.6 %all-to-all-start.3 = ((bf16[64,32,256]{2,1,0:T(8,128)(2,1)}), bf16[64,32,256]{2,1,0:T(8,128)(2,1)}, u32[]{:S(2)}, u32[]{:S(2)}) async-start(bf16[64,32,256]{2,1,0:T(8,128)(2,1)} %bitcast.163), calls=%async_computation.3 | async-start | bytes 2097152 | tf_op jit(solution)/shard_map/all_to_all | solution.py:15
  244.9 3.1 %fusion.33 = bf16[1,2048,256]{1,2,0:T(8,128)(2,1)} fusion(bf16[64,1,12,2048]{3,0,2,1:T(8,128)(2,1)S(1)} %copy-done, bf16[64,1,12,256]{3,0,2,1:T(8,128)(2,1)} %copy-done.12), kind=kOutput, calls=%fused_computation.25 | convolution fusion | flops 805830656 | bytes 4587520 | tf_op jit(solution)/shard_map/secd,secf->edf/dot_general | solution.py:77
  248.0 2.0 fusion.30
  250.6 2.4 collective-permute-start.1
  253.1 2.0 fusion.36
  255.1 2.3 copy.55
  257.4 2.3 copy.56
  261.0 11.9 %all-to-all-done.3 = bf16[64,32,256]{2,1,0:T(8,128)(2,1)} async-done(((bf16[64,32,256]{2,1,0:T(8,128)(2,1)}), bf16[64,32,256]{2,1,0:T(8,128)(2,1)}, u32[]{:S(2)}, u32[]{:S(2)}) %all-to-all-start.3) | async-done | bytes 1048608 | tf_op jit(solution)/shard_map/all_to_all | solution.py:15
  272.9 2.0 convert_reduce_fusion
  (76 shorter events, 12.9 us)
Async XLA Ops:
  7.2 71.7 %copy-start = (bf16[64,1,12,2048]{3,0,2,1:T(8,128)(2,1)S(1)}, bf16[64,1,12,2048]{3,0,2,1:T(8,128)(2,1)}, u32[]{:S(2)}) copy-start(bf16[64,1,12,2048]{3,0,2,1:T(8,128)(2,1)} %param.15) | copy-start | bytes 9437188
  7.2 110.6 %all-gather.2.cloned.1.call-start = ((), (), s32[]{:S(2)}) async-start(), calls=%async_computation.4 | async-start | bytes 3932160 | tf_op jit(solution)/shard_map/all_gather | solution.py:64
  15.1 5.3 %copy-start.16 = (f32[192,2]{0,1:T(2,128)S(1)}, f32[192,2]{0,1:T(2,128)}, u32[]{:S(2)}) copy-start(f32[192,2]{0,1:T(2,128)} %param.14) | copy-start | bytes 4612
  78.9 3.2 %copy-start.2 = (bf16[1,2048,256]{2,1,0:T(8,128)(2,1)S(1)}, bf16[1,2048,256]{2,1,0:T(8,128)(2,1)}, u32[]{:S(2)}) copy-start(bf16[1,2048,256]{2,1,0:T(8,128)(2,1)} %param.17) | copy-start | bytes 3145732
  117.8 3.9 %copy-start.1 = (bf16[1,2048,256]{2,1,0:T(8,128)(2,1)S(1)}, bf16[1,2048,256]{2,1,0:T(8,128)(2,1)}, u32[]{:S(2)}) copy-start(bf16[1,2048,256]{2,1,0:T(8,128)(2,1)} %param.16) | copy-start | bytes 3145732
  121.7 1.1 copy-start.12
  121.7 1.1 copy-start.10
  121.7 1.5 copy-start.3
  164.5 18.2 %copy-start.5 = (bf16[192,256]{1,0:T(8,128)(2,1)S(1)}, bf16[192,256]{1,0:T(8,128)(2,1)}, u32[]{:S(2)}) copy-start(bf16[192,256]{1,0:T(8,128)(2,1)} %param.19) | copy-start | bytes 294916
  164.5 18.2 %copy-start.7 = (bf16[192,256]{1,0:T(8,128)(2,1)S(1)}, bf16[192,256]{1,0:T(8,128)(2,1)}, u32[]{:S(2)}) copy-start(bf16[192,256]{1,0:T(8,128)(2,1)} %param.21) | copy-start | bytes 294916
  164.5 22.0 %copy-start.13 = (s32[192,2]{0,1:T(2,128)S(1)}, s32[192,2]{0,1:T(2,128)}, u32[]{:S(2)}) copy-start(s32[192,2]{0,1:T(2,128)} %param.13) | copy-start | bytes 4612
  164.5 22.1 %copy-start.15 = (f32[3,256]{1,0:T(4,128)S(1)}, f32[3,256]{1,0:T(4,128)}, u32[]{:S(2)}) copy-start(f32[3,256]{1,0:T(4,128)} %param.22) | copy-start | bytes 9220
  170.6 40.2 %all-to-all-start.2 = ((bf16[64,1,12,512]{3,2,1,0:T(8,128)(2,1)}), bf16[64,1,12,512]{3,2,1,0:T(8,128)(2,1)}, u32[]{:S(2)}, u32[]{:S(2)}) async-start(bf16[64,1,12,512]{3,2,1,0:T(8,128)(2,1)} %copy.54), calls=%async_computation.2 | async-start | bytes 2097152 | tf_op jit(solution)/shard_map/all_to_all | solution.py:90
  182.8 5.3 %collective-permute-start = (bf16[2,2,256]{2,1,0:T(2,128)(2,1)S(1)}, bf16[2,2,256]{2,1,0:T(2,128)(2,1)S(1)}, u32[]{:S(2)}, u32[]{:S(2)}) collective-permute-start(bf16[2,2,256]{2,1,0:T(2,128)(2,1)S(1)} %pad_maximum_fusion.2), channel_id=1, source_target_pairs={{0,4},{4,8},{8,12},{12,16},{16,20},{20,24},{24,28},{28,32},{32,36}... | collective-permute-start | bytes 6152 | tf_op jit(solution)/shard_map/ppermute | solution.py:22
  216.2 15.1 %copy-start.14 = (f32[2,256]{1,0:T(2,128)S(1)}, f32[2,256]{1,0:T(2,128)}, u32[]{:S(2)}) copy-start(f32[2,256]{1,0:T(2,128)} %multiply_bitcast_fusion) | copy-start | bytes 6148
  217.1 16.6 %copy-start.9 = (bf16[192,256]{1,0:T(8,128)(2,1)S(1)}, bf16[192,256]{1,0:T(8,128)(2,1)}, u32[]{:S(2)}) copy-start(bf16[192,256]{1,0:T(8,128)(2,1)} %param.20) | copy-start | bytes 294916
  220.3 14.9 %copy-start.4 = (bf16[192,512]{1,0:T(8,128)(2,1)}, bf16[192,512]{1,0:T(8,128)(2,1)S(1)}, u32[]{:S(2)}) copy-start(bf16[192,512]{1,0:T(8,128)(2,1)S(1)} %add_convert_fusion.1) | copy-start | bytes 589828
  235.2 37.7 %all-to-all-start.3 = ((bf16[64,32,256]{2,1,0:T(8,128)(2,1)}), bf16[64,32,256]{2,1,0:T(8,128)(2,1)}, u32[]{:S(2)}, u32[]{:S(2)}) async-start(bf16[64,32,256]{2,1,0:T(8,128)(2,1)} %bitcast.163), calls=%async_computation.3 | async-start | bytes 2097152 | tf_op jit(solution)/shard_map/all_to_all | solution.py:15
  244.9 3.2 %copy-start.17 = (bf16[64,1,12,2048]{3,0,1,2:T(8,128)(2,1)S(1)}, bf16[64,1,12,2048]{3,0,1,2:T(8,128)(2,1)}, u32[]{:S(2)}) copy-start(bf16[64,1,12,2048]{3,0,1,2:T(8,128)(2,1)} %all-gather.2.cloned.1.call-done) | copy-start | bytes 9437188
  244.9 3.1 %copy-start.18 = (f32[64,1,12,256]{3,0,2,1:T(8,128)S(1)}, f32[64,1,12,256]{3,0,2,1:T(8,128)}, u32[]{:S(2)}) copy-start(f32[64,1,12,256]{3,0,2,1:T(8,128)} %fusion.48) | copy-start | bytes 2359300
  244.9 3.1 %copy-start.19 = (f32[64,1,12,256]{3,0,2,1:T(8,128)S(1)}, f32[64,1,12,256]{3,0,2,1:T(8,128)}, u32[]{:S(2)}) copy-start(f32[64,1,12,256]{3,0,2,1:T(8,128)} %fusion.45) | copy-start | bytes 2359300
  248.0 5.1 %copy-start.11 = (bf16[64,1,12,256]{3,0,2,1:T(8,128)(2,1)S(1)}, bf16[64,1,12,256]{3,0,2,1:T(8,128)(2,1)}, u32[]{:S(2)}) copy-start(bf16[64,1,12,256]{3,0,2,1:T(8,128)(2,1)} %copy-done.10) | copy-start | bytes 1179652
  250.6 9.0 %collective-permute-start.1 = (f32[2,256]{1,0:T(2,128)}, f32[2,256]{1,0:T(2,128)S(1)}, u32[]{:S(2)}, u32[]{:S(2)}) collective-permute-start(f32[2,256]{1,0:T(2,128)} %slice.66), channel_id=1, source_target_pairs={{4,0},{8,4},{12,8},{16,12},{20,16},{24,20},{28,24},{32,28},{36,32}... | collective-permute-start | bytes 6152 | tf_op jit(solution)/shard_map/ppermute | solution.py:22
  255.1 4.6 %copy-start.6 = (bf16[192,256]{1,0:T(8,128)(2,1)S(1)}, bf16[192,256]{1,0:T(8,128)(2,1)}, u32[]{:S(2)}) copy-start(bf16[192,256]{1,0:T(8,128)(2,1)} %param.19) | copy-start | bytes 294916
  255.1 5.3 %copy-start.8 = (bf16[192,256]{1,0:T(8,128)(2,1)S(1)}, bf16[192,256]{1,0:T(8,128)(2,1)}, u32[]{:S(2)}) copy-start(bf16[192,256]{1,0:T(8,128)(2,1)} %param.21) | copy-start | bytes 294916
Sparse Core Ops, SparseCore 0:
  79.0 38.7 all-gather.1
where the time goes:
time: 283 us; the launch traced here: 282 us
  blocking collectives  92 us (33%)
  waiting for transfers between devices  67.9 us (24%)
  local copies, waits for them, and re-layouts  37.9 us (13%)
  starting transfers between devices  27.8 us (10%)
  matrix products  22 us (8%)
  other arithmetic  19.7 us (7%)
  between operations  14.4 us (5%)
    all_to_all x1, blocking collectives, on_device(): lax.all_to_all(piece, 'sp', split_axis=0, concat_axis=0, tiled=True)  41.1 us
    all_to_all x1, blocking collectives, sum_at_owner(): pieces = lax.all_to_all(split_up(shard, dim, peers), axis, 0, 0, tiled=True)  39.9 us
    all_gather x1, waiting for transfers between devices, on_device(): grads = lax.all_gather(arrived, 'tp', axis=2, tiled=True)  33.8 us
    all_to_all x1, waiting for transfers between devices, on_device(): lax.all_to_all(summed.astype(jnp.bfloat16), 'sp', split_axis=0, concat_ax...  22.2 us
    all_to_all x1, starting transfers between devices, on_device(): lax.all_to_all(summed.astype(jnp.bfloat16), 'sp', split_axis=0, concat_ax...  12.1 us
    all_to_all x1, waiting for transfers between devices, sum_at_owner(): pieces = lax.all_to_all(split_up(shard, dim, peers), axis, 0, 0, tiled=True)  11.9 us
    all_gather x1, blocking collectives, on_device(): mid_whole = lax.all_gather(mid_grad, 'tp', axis=1, tiled=True)  11 us
    mul x3, local copies, waits for them, and re-layouts, on_device(): route_weight[:, :, None] * out_grad[:, None, :].astype(jnp.float32)  9.84 us
  transfers between devices with their start and end apart: 5, of which 3 were waited for; matrix products, arithmetic and copies ran while one was open for 7% of the time, Pallas kernels for 0%

commit v1 on v0

--- a/solution.py
+++ b/solution.py
@@ -1,7 +1,36 @@
+import functools
 import jax
 import jax.numpy as jnp
 from jax import lax
 from jax.sharding import PartitionSpec as P
+
+
+def put_types_for(array_here, along_axis, dim_k):
+    v1, x_next, w1 = (
+        jax.lax.axis_size(along_axis),
+        jax.lax.axis_index(along_axis),
+        array_here.shape[dim_k],
+    )
+    grid = tuple(((num, (num + 1) % v1) for num in range(v1)))
+    chunks = tuple(((num, (num - 1) % v1) for num in range(v1)))
+    upper = jnp.zeros(
+        (*array_here.shape[:dim_k], v1 * w1, *array_here.shape[dim_k + 1 :]), array_here.dtype
+    )
+    upper = lax.dynamic_update_slice_in_dim(upper, array_here, x_next * w1, axis=dim_k)
+    big = work_now = array_here
+    even = v1 // 2
+    for c in range(1, even + 1):
+        big = jax.lax.ppermute(big, along_axis, grid)
+        upper = lax.dynamic_update_slice_in_dim(upper, big, (x_next - c) % v1 * w1, axis=dim_k)
+        if c < v1 - even:
+            work_now = jax.lax.ppermute(work_now, along_axis, chunks)
+            upper = lax.dynamic_update_slice_in_dim(
+                upper, work_now, (x_next + c) % v1 * w1, axis=dim_k
+            )
+    return upper
+
+
+serve_edge = functools.partial(put_types_for, along_axis="tp", dim_k=2)
 
 
 def split_up(shard, dim, peers):
@@ -61,7 +90,7 @@
     portion = slots // groups
     piece = lax.dynamic_slice_in_dim(outgoing, member * portion, portion, 2)
     arrived = lax.all_to_all(piece, "sp", split_axis=0, concat_axis=0, tiled=True)
-    grads = lax.all_gather(arrived, "tp", axis=2, tiled=True)
+    grads = serve_edge(arrived)
     gate = jnp.einsum(
         "secd,edf->secf", expert_rows, gate_weight, preferred_element_type=jnp.float32
     )

time: 283 us -> 265 us (0.936)
  blocking collectives: 92 us -> 48.8 us
  waiting for transfers between devices: 67.9 us -> 88.8 us
  starting transfers between devices: 27.8 us -> 43.5 us
  between operations: 14.4 us -> 1.12 us
  local copies, waits for them, and re-layouts: 37.9 us -> 42.4 us
    all_to_all x1 -> x0, blocking collectives: 41.1 us -> none  [on_device(): lax.all_to_all(piece, 'sp', split_axis=0, concat_axis=0, tiled=True)]
    all_gather x1 -> x0, waiting for transfers between devices: 33.8 us -> none  [on_device(): grads = lax.all_gather(arrived, 'tp', axis=2, tiled=True)]
    ppermute x0 -> x3, waiting for transfers between devices: none -> 29.8 us  [the longest x2 27.6 us: put_types_for(): big = jax.lax.ppermute(big, along_axis, grid)]
    all_to_all x0 -> x1, waiting for transfers between devices: none -> 24.9 us  [on_device(): lax.all_to_all(piece, 'sp', split_axis=0, concat_axis=0, tiled=True)]
    all_to_all x0 -> x1, starting transfers between devices: none -> 13.3 us  [on_device(): lax.all_to_all(piece, 'sp', split_axis=0, concat_axis=0, tiled=True)]
    ppermute x0 -> x3, starting transfers between devices: none -> 3.01 us  [the longest x1 1.72 us: put_types_for(): work_now = jax.lax.ppermute(work_now, along_axis, chunks)]
    unnamed x44 -> x50, local copies, waits for them, and re-layouts: 6.07 us -> 6.65 us
  transfers between devices with their start and end apart: 5 -> 8, of which waited for: 3 -> 6; matrix products, arithmetic and copies ran while one was open for 7% -> 9% of each run, Pallas kernels for 0% -> 0%
where the time goes in v1:
time: 265 us; the launch traced here: 264 us
  waiting for transfers between devices  88.8 us (34%)
  blocking collectives  48.8 us (18%)
  starting transfers between devices  43.5 us (16%)
  local copies, waits for them, and re-layouts  42.4 us (16%)
  other arithmetic  19.8 us (7%)
  matrix products  19.6 us (7%)
    all_to_all x1, blocking collectives, sum_at_owner(): pieces = lax.all_to_all(split_up(shard, dim, peers), axis, 0, 0, tiled=True)  37.9 us
    ppermute x2, waiting for transfers between devices, put_types_for(): big = jax.lax.ppermute(big, along_axis, grid)  27.6 us
    all_to_all x1, waiting for transfers between devices, on_device(): lax.all_to_all(piece, 'sp', split_axis=0, concat_axis=0, tiled=True)  24.9 us
    all_to_all x1, waiting for transfers between devices, on_device(): lax.all_to_all(summed.astype(jnp.bfloat16), 'sp', split_axis=0, concat_ax...  22.2 us
    all_to_all x1, starting transfers between devices, on_device(): lax.all_to_all(piece, 'sp', split_axis=0, concat_axis=0, tiled=True)  13.3 us
    all_to_all x1, waiting for transfers between devices, sum_at_owner(): pieces = lax.all_to_all(split_up(shard, dim, peers), axis, 0, 0, tiled=True)  11.9 us
    all_to_all x1, starting transfers between devices, on_device(): lax.all_to_all(summed.astype(jnp.bfloat16), 'sp', split_axis=0, concat_ax...  11.5 us
    all_gather x1, blocking collectives, on_device(): mid_whole = lax.all_gather(mid_grad, 'tp', axis=1, tiled=True)  11 us
  transfers between devices with their start and end apart: 8, of which 6 were waited for; matrix products, arithmetic and copies ran while one was open for 9% of the time, Pallas kernels for 0%

profile of v1, /device:TPU:1, one launch (start us, length us, event | category | flops | bytes accessed | tf_op | source)
XLA Modules:
  0.0 263.9 jit_solution(18041572222220663740)
XLA Ops:
  4.2 4.4 %mul.158 = f32[192,2,2048]{2,1,0:T(2,128)} broadcast(bf16[192,2048]{1,0:T(8,128)(2,1)} %param.12), dimensions={0,2} | broadcast | bytes 3932160 | tf_op jit(solution)/shard_map/mul | solution.py:81
  8.6 5.3 %mul.159 = f32[384,2048]{1,0:T(8,128)} reshape(f32[192,2,2048]{2,1,0:T(2,128)} %mul.158) | data formatting | bytes 6291456 | tf_op jit(solution)/shard_map/mul | solution.py:81
  14.2 6.4 %scatter_custom_fusion = bf16[768,2048]{1,0:T(8,128)(2,1)} fusion(s32[384]{0:T(512)S(1)} %fusion.66, f32[384,2048]{1,0:T(8,128)} %mul.159, f32[384]{0:T(512)S(1)} %mul.156, bf16[]{:T(256)} %constant.58.clone.1), kind=kCustom, calls=%fused_computation.24 | custom fusion | flops 1572864 | bytes 6293506 | tf_op jit(solution)/shard_map/scatter | solution.py:87
  20.6 6.0 %reshape.159 = bf16[64,1,12,2048]{3,2,0,1:T(8,128)(2,1)} reshape(bf16[768,2048]{1,0:T(8,128)(2,1)} %scatter_custom_fusion) | data formatting | bytes 6291456 | tf_op jit(solution)/shard_map/reshape | solution.py:89
  26.7 4.0 %dynamic-slice_bitcast_fusion = bf16[64,1,3,2048]{3,2,1,0:T(4,128)(2,1)} fusion(bf16[64,1,12,2048]{3,2,0,1:T(8,128)(2,1)} %reshape.159, s32[]{:T(128)S(6)} %select_n.55), kind=kLoop, calls=%fused_computation.36 | loop fusion | bytes 1572868 | tf_op jit(solution)/shard_map/dynamic_slice | solution.py:91
  30.7 13.3 %all-to-all-start = ((bf16[64,1,3,2048]{3,2,1,0:T(4,128)(2,1)}), bf16[64,1,3,2048]{3,2,1,0:T(4,128)(2,1)}, u32[]{:S(2)}, u32[]{:S(2)}) async-start(bf16[64,1,3,2048]{3,2,1,0:T(4,128)(2,1)} %dynamic-slice_bitcast_fusion), calls=%async_computation | async-start | bytes 2097152 | tf_op jit(solution)/shard_map/all_to_all | solution.py:92
  44.1 3.1 %fusion.34 = f32[64,1,12,256]{3,0,2,1:T(8,128)} fusion(bf16[64,1,12,2048]{3,0,2,1:T(8,128)(2,1)S(1)} %copy-done, bf16[1,2048,256]{2,1,0:T(8,128)(2,1)} %param.16), kind=kOutput, calls=%fused_computation.28 | convolution fusion | flops 805306368 | bytes 4980736 | tf_op jit(solution)/shard_map/secd,edf->secf/dot_general | solution.py:94
  47.2 24.9 %all-to-all-done = bf16[64,1,3,2048]{3,2,1,0:T(4,128)(2,1)} async-done(((bf16[64,1,3,2048]{3,2,1,0:T(4,128)(2,1)}), bf16[64,1,3,2048]{3,2,1,0:T(4,128)(2,1)}, u32[]{:S(2)}, u32[]{:S(2)}) %all-to-all-start) | async-done | bytes 786464 | tf_op jit(solution)/shard_map/all_to_all | solution.py:92
  75.2 2.2 fusion.31
  79.5 2.0 copy_dynamic-update-slice_fusion
  81.5 11.6 %collective-permute-done = bf16[64,1,3,2048]{3,0,2,1:T(8,128)(2,1)S(1)} collective-permute-done((bf16[64,1,3,2048]{3,0,2,1:T(8,128)(2,1)S(1)}, bf16[64,1,3,2048]{3,0,2,1:T(8,128)(2,1)S(1)}, u32[]{:S(2)}, u32[]{:S(2)}) %collective-permute-start) | collective-permute-done | bytes 786464 | tf_op jit(solution)/shard_map/ppermute | solution.py:23
  93.2 2.1 collective-permute-done.1
  95.4 16.0 %collective-permute-done.2 = bf16[64,1,3,2048]{3,0,2,1:T(8,128)(2,1)S(1)} collective-permute-done((bf16[64,1,3,2048]{3,0,2,1:T(8,128)(2,1)S(1)}, bf16[64,1,3,2048]{3,0,2,1:T(8,128)(2,1)S(1)}, u32[]{:S(2)}, u32[]{:S(2)}) %collective-permute-start.2) | collective-permute-done | bytes 786464 | tf_op jit(solution)/shard_map/ppermute | solution.py:23
  116.2 37.9 %all_to_all.20 = bf16[4,64,1,12,512]{4,1,3,2,0:T(8,128)(2,1)} all-to-all(bf16[4,64,1,12,512]{4,1,3,2,0:T(8,128)(2,1)S(1)} %bitcast.155), channel_id=1, replica_groups=mesh['sp'=64,'tp'=4] {'tp'}, dimensions={0} | all-to-all | bytes 6291456 | tf_op jit(solution)/shard_map/all_to_all | solution.py:44
  154.1 3.5 %reduce_sum.48 = bf16[64,12,512]{2,0,1:T(8,128)(2,1)} reduce(bf16[4,64,1,12,512]{4,1,3,2,0:T(8,128)(2,1)} %all_to_all.20, bf16[]{:T(256)} %constant.58.clone.1), dimensions={0,2}, to_apply=%region_4.5 | reduce | flops 1179648 | bytes 3932162 | tf_op jit(solution)/shard_map/reduce_sum | solution.py:45
  157.6 2.5 copy.61
  160.1 11.5 %all-to-all-start.2 = ((bf16[64,1,12,512]{3,2,1,0:T(8,128)(2,1)}), bf16[64,1,12,512]{3,2,1,0:T(8,128)(2,1)}, u32[]{:S(2)}, u32[]{:S(2)}) async-start(bf16[64,1,12,512]{3,2,1,0:T(8,128)(2,1)} %copy.61), calls=%async_computation.2 | async-start | bytes 2097152 | tf_op jit(solution)/shard_map/all_to_all | solution.py:119
  171.7 3.5 %collective-permute-start.3 = (bf16[2,2,256]{2,1,0:T(2,128)(2,1)S(1)}, bf16[2,2,256]{2,1,0:T(2,128)(2,1)S(1)}, u32[]{:S(2)}, u32[]{:S(2)}) collective-permute-start(bf16[2,2,256]{2,1,0:T(2,128)(2,1)S(1)} %pad_maximum_fusion.2), channel_id=1, source_target_pairs={{0,4},{4,8},{8,12},{12,16},{16,20},{20,24},{24,28},{28,32},{32,36}... | collective-permute-start | bytes 6152 | tf_op jit(solution)/shard_map/ppermute | solution.py:51
  177.6 22.2 %all-to-all-done.2 = bf16[64,1,12,512]{3,2,1,0:T(8,128)(2,1)} async-done(((bf16[64,1,12,512]{3,2,1,0:T(8,128)(2,1)}), bf16[64,1,12,512]{3,2,1,0:T(8,128)(2,1)}, u32[]{:S(2)}, u32[]{:S(2)}) %all-to-all-start.2) | async-done | bytes 786464 | tf_op jit(solution)/shard_map/all_to_all | solution.py:119
  199.8 2.1 reshape.172
  201.8 3.3 %gather_fusion = bf16[384,512]{1,0:T(8,128)(2,1)S(1)} fusion(bf16[768,512]{1,0:T(8,128)(2,1)} %reshape.172, s32[1024]{0:T(1024)S(1)} %pad_clamp_fusion), kind=kCustom, calls=%fused_computation | custom fusion | bytes 787968 | tf_op jit(solution)/shard_map/jit(_take)/gather | solution.py:124
  206.1 2.2 convert_reduce_fusion.1
  209.3 11.0 %all_gather.3 = bf16[192,2048]{1,0:T(8,128)(2,1)S(1)} all-gather(bf16[192,512]{1,0:T(8,128)(2,1)S(1)} %add_convert_fusion.1), channel_id=1, replica_groups=mesh['sp'=64,'tp'=4] {'tp'}, dimensions={1}, use_global_device_ids=true | all-gather | bytes 983040 | tf_op jit(solution)/shard_map/all_gather | solution.py:131
  220.2 2.5 multiply_convert_fusion.6
  224.2 9.6 %all-to-all-start.3 = ((bf16[64,32,256]{2,1,0:T(8,128)(2,1)}), bf16[64,32,256]{2,1,0:T(8,128)(2,1)}, u32[]{:S(2)}, u32[]{:S(2)}) async-start(bf16[64,32,256]{2,1,0:T(8,128)(2,1)} %bitcast.157), calls=%async_computation.3 | async-start | bytes 2097152 | tf_op jit(solution)/shard_map/all_to_all | solution.py:44
  233.8 3.1 %fusion.21 = bf16[1,2048,256]{1,2,0:T(8,128)(2,1)} fusion(bf16[64,1,12,2048]{3,0,2,1:T(8,128)(2,1)S(1)} %copy-done, bf16[64,1,12,256]{3,0,2,1:T(8,128)(2,1)} %copy-done.13), kind=kOutput, calls=%fused_computation.20 | convolution fusion | flops 805830656 | bytes 4587520 | tf_op jit(solution)/shard_map/secd,secf->edf/dot_general | solution.py:106
  237.0 2.0 fusion.27
  239.6 2.4 collective-permute-start.4
  244.0 2.3 copy.62
  246.3 2.3 copy.63
  250.0 11.9 %all-to-all-done.3 = bf16[64,32,256]{2,1,0:T(8,128)(2,1)} async-done(((bf16[64,32,256]{2,1,0:T(8,128)(2,1)}), bf16[64,32,256]{2,1,0:T(8,128)(2,1)}, u32[]{:S(2)}, u32[]{:S(2)}) %all-to-all-start.3) | async-done | bytes 1048608 | tf_op jit(solution)/shard_map/all_to_all | solution.py:44
  261.9 2.0 convert_reduce_fusion
  (91 shorter events, 23.5 us)
Async XLA Ops:
  0.6 43.4 %copy-start = (bf16[64,1,12,2048]{3,0,2,1:T(8,128)(2,1)S(1)}, bf16[64,1,12,2048]{3,0,2,1:T(8,128)(2,1)}, u32[]{:S(2)}) copy-start(bf16[64,1,12,2048]{3,0,2,1:T(8,128)(2,1)} %param.15) | copy-start | bytes 9437188
  8.6 5.3 %copy-start.17 = (f32[192,2]{0,1:T(2,128)S(1)}, f32[192,2]{0,1:T(2,128)}, u32[]{:S(2)}) copy-start(f32[192,2]{0,1:T(2,128)} %param.14) | copy-start | bytes 4612
  30.7 41.4 %all-to-all-start = ((bf16[64,1,3,2048]{3,2,1,0:T(4,128)(2,1)}), bf16[64,1,3,2048]{3,2,1,0:T(4,128)(2,1)}, u32[]{:S(2)}, u32[]{:S(2)}) async-start(bf16[64,1,3,2048]{3,2,1,0:T(4,128)(2,1)} %dynamic-slice_bitcast_fusion), calls=%async_computation | async-start | bytes 2097152 | tf_op jit(solution)/shard_map/all_to_all | solution.py:92
  73.9 19.2 %collective-permute-start = (bf16[64,1,3,2048]{3,0,2,1:T(8,128)(2,1)S(1)}, bf16[64,1,3,2048]{3,0,2,1:T(8,128)(2,1)S(1)}, u32[]{:S(2)}, u32[]{:S(2)}) collective-permute-start(bf16[64,1,3,2048]{3,0,2,1:T(8,128)(2,1)S(1)} %copy.55), channel_id=1, source_target_pairs={{0,1},{1,2},{2,3},{3,0},{4,5},{5,6},{6,7},{7,4},{8,9},{9,10},{10,1... | collective-permute-start | bytes 2359304 | tf_op jit(solution)/shard_map/ppermute | solution.py:23
  77.4 34.1 %copy-start.21 = (f32[64,1,12,256]{3,0,2,1:T(8,128)}, f32[64,1,12,256]{3,0,2,1:T(8,128)S(1)}, u32[]{:S(2)}) copy-start(f32[64,1,12,256]{3,0,2,1:T(8,128)S(1)} %fusion.31) | copy-start | bytes 2359300
  77.4 17.9 %collective-permute-start.1 = (bf16[64,1,3,2048]{3,0,2,1:T(8,128)(2,1)S(1)}, bf16[64,1,3,2048]{3,0,2,1:T(8,128)(2,1)S(1)}, u32[]{:S(2)}, u32[]{:S(2)}) collective-permute-start(bf16[64,1,3,2048]{3,0,2,1:T(8,128)(2,1)S(1)} %copy.55), channel_id=1, source_target_pairs={{0,3},{1,0},{2,1},{3,2},{4,7},{5,4},{6,5},{7,6},{8,11},{9,8},{10,9... | collective-permute-start | bytes 2359304 | tf_op jit(solution)/shard_map/ppermute | solution.py:26
  79.5 32.0 %copy-start.18 = (bf16[1,256,2048]{2,1,0:T(8,128)(2,1)S(1)}, bf16[1,256,2048]{2,1,0:T(8,128)(2,1)}, u32[]{:S(2)}) copy-start(bf16[1,256,2048]{2,1,0:T(8,128)(2,1)} %param.18) | copy-start | bytes 3145732
  79.5 32.0 %copy-start.19 = (f32[64,1,12,256]{3,0,2,1:T(8,128)S(1)}, f32[64,1,12,256]{3,0,2,1:T(8,128)}, u32[]{:S(2)}) copy-start(f32[64,1,12,256]{3,0,2,1:T(8,128)} %fusion.34) | copy-start | bytes 2359300
  93.1 18.3 %collective-permute-start.2 = (bf16[64,1,3,2048]{3,0,2,1:T(8,128)(2,1)S(1)}, bf16[64,1,3,2048]{3,0,2,1:T(8,128)(2,1)S(1)}, u32[]{:S(2)}, u32[]{:S(2)}) collective-permute-start(bf16[64,1,3,2048]{3,0,2,1:T(8,128)(2,1)S(1)} %collective-permute-done), channel_id=1, source_target_pairs={{0,1},{1,2},{2,3},{3,0},{4,5},{5,6},{6,7},{7,4},{8,9},{9,10},{10,1... | collective-permute-start | bytes 2359304 | tf_op jit(solution)/shard_map/ppermute | solution.py:23
  111.6 1.6 copy-start.1
  111.6 2.0 copy-start.3
  113.2 1.4 copy-start.13
  113.2 1.4 copy-start.11
  113.6 1.2 copy-start.4
  154.1 17.6 %copy-start.6 = (bf16[192,256]{1,0:T(8,128)(2,1)S(1)}, bf16[192,256]{1,0:T(8,128)(2,1)}, u32[]{:S(2)}) copy-start(bf16[192,256]{1,0:T(8,128)(2,1)} %param.19) | copy-start | bytes 294916
  154.1 17.6 %copy-start.8 = (bf16[192,256]{1,0:T(8,128)(2,1)S(1)}, bf16[192,256]{1,0:T(8,128)(2,1)}, u32[]{:S(2)}) copy-start(bf16[192,256]{1,0:T(8,128)(2,1)} %param.21) | copy-start | bytes 294916
  154.1 21.5 %copy-start.14 = (s32[192,2]{0,1:T(2,128)S(1)}, s32[192,2]{0,1:T(2,128)}, u32[]{:S(2)}) copy-start(s32[192,2]{0,1:T(2,128)} %param.13) | copy-start | bytes 4612
  154.1 21.5 %copy-start.16 = (f32[3,256]{1,0:T(4,128)S(1)}, f32[3,256]{1,0:T(4,128)}, u32[]{:S(2)}) copy-start(f32[3,256]{1,0:T(4,128)} %param.22) | copy-start | bytes 9220
  160.1 39.6 %all-to-all-start.2 = ((bf16[64,1,12,512]{3,2,1,0:T(8,128)(2,1)}), bf16[64,1,12,512]{3,2,1,0:T(8,128)(2,1)}, u32[]{:S(2)}, u32[]{:S(2)}) async-start(bf16[64,1,12,512]{3,2,1,0:T(8,128)(2,1)} %copy.61), calls=%async_computation.2 | async-start | bytes 2097152 | tf_op jit(solution)/shard_map/all_to_all | solution.py:119
  171.7 5.3 %collective-permute-start.3 = (bf16[2,2,256]{2,1,0:T(2,128)(2,1)S(1)}, bf16[2,2,256]{2,1,0:T(2,128)(2,1)S(1)}, u32[]{:S(2)}, u32[]{:S(2)}) collective-permute-start(bf16[2,2,256]{2,1,0:T(2,128)(2,1)S(1)} %pad_maximum_fusion.2), channel_id=1, source_target_pairs={{0,4},{4,8},{8,12},{12,16},{16,20},{20,24},{24,28},{28,32},{32,36}... | collective-permute-start | bytes 6152 | tf_op jit(solution)/shard_map/ppermute | solution.py:51
  205.2 15.1 %copy-start.15 = (f32[2,256]{1,0:T(2,128)S(1)}, f32[2,256]{1,0:T(2,128)}, u32[]{:S(2)}) copy-start(f32[2,256]{1,0:T(2,128)} %multiply_bitcast_fusion) | copy-start | bytes 6148
  206.1 16.6 %copy-start.10 = (bf16[192,256]{1,0:T(8,128)(2,1)S(1)}, bf16[192,256]{1,0:T(8,128)(2,1)}, u32[]{:S(2)}) copy-start(bf16[192,256]{1,0:T(8,128)(2,1)} %param.20) | copy-start | bytes 294916
  209.3 14.9 %copy-start.5 = (bf16[192,512]{1,0:T(8,128)(2,1)}, bf16[192,512]{1,0:T(8,128)(2,1)S(1)}, u32[]{:S(2)}) copy-start(bf16[192,512]{1,0:T(8,128)(2,1)S(1)} %add_convert_fusion.1) | copy-start | bytes 589828
  224.2 37.7 %all-to-all-start.3 = ((bf16[64,32,256]{2,1,0:T(8,128)(2,1)}), bf16[64,32,256]{2,1,0:T(8,128)(2,1)}, u32[]{:S(2)}, u32[]{:S(2)}) async-start(bf16[64,32,256]{2,1,0:T(8,128)(2,1)} %bitcast.157), calls=%async_computation.3 | async-start | bytes 2097152 | tf_op jit(solution)/shard_map/all_to_all | solution.py:44
  233.8 3.2 %copy-start.2 = (bf16[64,12,2048]{2,0,1:T(8,128)(2,1)S(1)}, bf16[64,12,2048]{2,0,1:T(8,128)(2,1)}, u32[]{:S(2)}) copy-start(bf16[64,12,2048]{2,0,1:T(8,128)(2,1)} %copy-done.1) | copy-start | bytes 9437188
  233.8 3.1 %copy-start.20 = (f32[64,1,12,256]{3,0,2,1:T(8,128)S(1)}, f32[64,1,12,256]{3,0,2,1:T(8,128)}, u32[]{:S(2)}) copy-start(f32[64,1,12,256]{3,0,2,1:T(8,128)} %fusion.34) | copy-start | bytes 2359300
  233.8 3.1 %copy-start.22 = (f32[64,1,12,256]{3,0,2,1:T(8,128)S(1)}, f32[64,1,12,256]{3,0,2,1:T(8,128)}, u32[]{:S(2)}) copy-start(f32[64,1,12,256]{3,0,2,1:T(8,128)} %copy-done.21) | copy-start | bytes 2359300
  237.0 5.1 %copy-start.12 = (bf16[64,1,12,256]{3,0,2,1:T(8,128)(2,1)S(1)}, bf16[64,1,12,256]{3,0,2,1:T(8,128)(2,1)}, u32[]{:S(2)}) copy-start(bf16[64,1,12,256]{3,0,2,1:T(8,128)(2,1)} %copy-done.11) | copy-start | bytes 1179652
  239.6 9.0 %collective-permute-start.4 = (f32[2,256]{1,0:T(2,128)}, f32[2,256]{1,0:T(2,128)S(1)}, u32[]{:S(2)}, u32[]{:S(2)}) collective-permute-start(f32[2,256]{1,0:T(2,128)} %slice.66), channel_id=1, source_target_pairs={{4,0},{8,4},{12,8},{16,12},{20,16},{24,20},{28,24},{32,28},{36,32}... | collective-permute-start | bytes 6152 | tf_op jit(solution)/shard_map/ppermute | solution.py:51
  244.0 4.6 %copy-start.7 = (bf16[192,256]{1,0:T(8,128)(2,1)S(1)}, bf16[192,256]{1,0:T(8,128)(2,1)}, u32[]{:S(2)}) copy-start(bf16[192,256]{1,0:T(8,128)(2,1)} %param.19) | copy-start | bytes 294916
  244.0 5.3 %copy-start.9 = (bf16[192,256]{1,0:T(8,128)(2,1)S(1)}, bf16[192,256]{1,0:T(8,128)(2,1)}, u32[]{:S(2)}) copy-start(bf16[192,256]{1,0:T(8,128)(2,1)} %param.21) | copy-start | bytes 294916
